TPU v7x, 32 devices: a whole 2x2x4 slice. The times are simulated.
32 devices in a mesh: sp: 8 (over z, y), tp: 4 (over x, core).
Axes of the slice: x: 2, y: 2, z: 4, core: 2. Of those that a mesh axis runs over, the one named last changes fastest.
Arguments:
- inputs: bfloat16 [2, 3072, 4096], P(None, 'sp'), may hold values from -8 to 8
- w_key: bfloat16 [4096, 2048], P(None, 'tp'), may hold values from -0.09375 to 0.09375
- w_value: bfloat16 [4096, 2048], P(None, 'tp'), may hold values from -0.09375 to 0.09375
- w_query: bfloat16 [4096, 2048], P(None, 'tp'), may hold values from -0.09375 to 0.09375
- w_igate: bfloat16 [4096, 16], replicated, may hold values from -1 to 1
- w_fgate: bfloat16 [4096, 16], replicated, may hold values from -0.09375 to 0.09375
- forget_bias: float32 [16], replicated, may hold values from 3 to 12
- new_rows: bfloat16 [2, 4096], P(None, 'tp'), may hold values from -6 to 6
Outputs:
- cache_matrix: bfloat16 [2, 16, 128, 128], P(None, 'tp', 'sp')
- cache_normal: float32 [2, 16, 128], P(None, 'tp', 'sp')
- cache_top: float32 [2, 16], P(None, 'tp')
- read: bfloat16 [2, 16, 128], P(None, 'tp', 'sp')
All inputs are finite; a program needn't handle non-finite values.
Results may differ from a plain program's by a relative error of at most 0.015.
Values may be sent and summed in bfloat16 or wider, within the bound.
A program may use at most 64 MiB of HBM per device.

v0:
```python
import jax
import jax.numpy as jnp
from jax import lax
from jax.sharding import PartitionSpec as P

DH = 128


EPS = 1e-06


def prefix(value, axis, combine, identity):
    devices, here = (lax.axis_size(axis), lax.axis_index(axis))
    everything = lax.all_gather(value, axis)
    start = jnp.broadcast_to(jnp.asarray(identity, value.dtype), value.shape)

    def lap(k, before):
        at = devices - 1 - k
        reached = at > here
        new = combine(before, everything[at])
        return jnp.where(reached, new, before)

    return lax.fori_loop(0, devices, lap, start)


def normalize(row_block):
    scaled = row_block.astype(jnp.float32)
    scaled = scaled * lax.rsqrt(jnp.mean(scaled * scaled, axis=-1, keepdims=True) + EPS)
    return scaled.astype(jnp.bfloat16)


def add_pair(earlier, second):
    return earlier + second


def shards(inputs, w_key, w_value, w_query, w_igate, w_fgate, forget_bias, new_rows):
    head_count = w_key.shape[1] // DH
    seq_count, span, width = inputs.shape
    rows_own = DH // lax.axis_size("sp")
    row_start = lax.axis_index("sp") * rows_own
    head_start = lax.axis_index("tp") * head_count
    gate_in = lax.dynamic_slice_in_dim(w_igate, head_start, head_count, 1)
    gate_forget = lax.dynamic_slice_in_dim(w_fgate, head_start, head_count, 1)
    bias_heads = lax.dynamic_slice_in_dim(forget_bias, head_start, head_count, 0)
    normed = normalize(inputs)
    key_rows = jnp.einsum("spd,dc->spc", normed, w_key, preferred_element_type=jnp.float32).astype(
        jnp.bfloat16
    )
    value_rows = jnp.einsum(
        "spd,dc->spc", normed, w_value, preferred_element_type=jnp.float32
    ).astype(jnp.bfloat16)
    input_pre = jnp.einsum("spd,dh->sph", normed, gate_in, preferred_element_type=jnp.float32)
    log_forget = jax.nn.log_sigmoid(
        jnp.einsum("spd,dh->sph", normed, gate_forget, preferred_element_type=jnp.float32)
        + bias_heads
    )
    running = jnp.cumsum(log_forget, axis=1)
    own_total = running[:, -1, :]
    beyond = prefix(own_total, "sp", add_pair, jnp.zeros_like(own_total))
    log_weight = (beyond + own_total)[:, None, :] - running + input_pre
    stabilizer = lax.pmax(jnp.max(log_weight, axis=1), "sp")
    weight = jnp.exp(log_weight - stabilizer[:, None, :])
    key_heads = key_rows.reshape(seq_count, span, head_count, DH)
    value_heads = value_rows.reshape(seq_count, span, head_count, DH)
    weighted = (weight[..., None] * value_heads.astype(jnp.float32)).astype(jnp.bfloat16)
    partial_normal = jnp.einsum("sth,sthd->shd", weight, key_heads.astype(jnp.float32))
    partial_matrix = jnp.einsum(
        "sthe,sthd->shed", weighted, key_heads, preferred_element_type=jnp.float32
    )
    matrix, normal = (
        lax.psum_scatter(partial_matrix, "sp", scatter_dimension=2, tiled=True),
        lax.psum_scatter(partial_normal, "sp", scatter_dimension=2, tiled=True),
    )
    cache_matrix = matrix.astype(jnp.bfloat16)
    new_normed = normalize(lax.all_gather(new_rows, "tp", axis=1, tiled=True))
    query_new = jnp.dot(new_normed, w_query, preferred_element_type=jnp.float32).astype(
        jnp.bfloat16
    )
    key_new = jnp.dot(new_normed, w_key, preferred_element_type=jnp.float32).astype(jnp.bfloat16)
    value_new = jnp.dot(new_normed, w_value, preferred_element_type=jnp.float32).astype(
        jnp.bfloat16
    )
    query_new = query_new.astype(jnp.float32).reshape(seq_count, head_count, DH)
    key_new = key_new.astype(jnp.float32).reshape(seq_count, head_count, DH)
    value_new = value_new.astype(jnp.float32).reshape(seq_count, head_count, DH)
    value_own = lax.dynamic_slice_in_dim(value_new, row_start, rows_own, 2)
    query_own = lax.dynamic_slice_in_dim(query_new, row_start, rows_own, 2)
    input_new = jnp.dot(new_normed, gate_in, preferred_element_type=jnp.float32)
    forget_new = jax.nn.log_sigmoid(
        jnp.dot(new_normed, gate_forget, preferred_element_type=jnp.float32) + bias_heads
    )
    top_next = jnp.maximum(forget_new + stabilizer, input_new)
    old_share = jnp.exp(forget_new + stabilizer - top_next)
    new_share = jnp.exp(input_new - top_next)
    agreement = jnp.sum(key_new * query_new, axis=-1)
    factor = DH ** (-0.5)
    numerator = old_share[..., None] * jnp.einsum(
        "shed,shd->she", cache_matrix.astype(jnp.float32), query_new
    )
    numerator = (numerator + (new_share * agreement)[..., None] * value_own) * factor
    normal_dot = lax.psum(jnp.sum(normal * query_own, axis=-1), "sp")
    denominator = (old_share * normal_dot + new_share * agreement) * factor
    read = numerator / jnp.maximum(jnp.abs(denominator), 1.0)[..., None]
    return (cache_matrix, normal, stabilizer, read.astype(jnp.bfloat16))


def solution(mesh):
    in_specs = (
        P(None, "sp", None),
        P(None, "tp"),
        P(None, "tp"),
        P(None, "tp"),
        P(),
        P(),
        P(),
        P(None, "tp"),
    )
    out_specs = (P(None, "tp", "sp", None), P(None, "tp", "sp"), P(None, "tp"), P(None, "tp", "sp"))
    return jax.shard_map(shards, mesh=mesh, in_specs=in_specs, out_specs=out_specs, check_vma=False)
```

profile of v0, /device:TPU:0, one launch (start us, length us, event | category | flops | bytes accessed | tf_op | source)
XLA Modules:
  0.0 208.2 jit_solution(13657243341448075160)
XLA Ops:
  7.2 0.0 copy-start
  7.2 0.0 copy-start.7
  7.2 0.0 reduce-scatter.7.cloned.1.call-start
  7.2 0.0 copy-start.6
  7.3 4.1 %fusion = f32[2,384]{1,0:T(2,128)S(1)} fusion(bf16[2,384,4096]{2,1,0:T(8,128)(2,1)} %param.10), kind=kLoop, calls=%fused_computation.3 | loop fusion | flops 9436416 | bytes 6294528 | tf_op jit(solution)/shard_map/reduce_sum | solution.py:28
  11.4 0.0 copy-done.7
  11.4 0.1 dynamic_slice.26
  11.5 0.0 copy-done
  11.5 4.6 %fusion.64 = f32[2,4,3,128]{3,1,2,0:T(4,128)S(1)} fusion(bf16[4096,16]{0,1:T(8,128)(2,1)S(1)} %copy-done, s32[]{:T(128)S(6)} %select_n.52, bf16[2,384,4096]{2,1,0:T(8,128)(2,1)} %param.10, f32[2,384]{1,0:T(2,128)S(1)} %add_rsqrt_fusion, f32[4]{0:T(128)S(1)} %dynamic_slice.26), kind=kOutput, calls=%fused_computation.47 | convolution fusion | flops 34630656 | bytes 6340100 | tf_op jit(solution)/shard_map/spd,dh->sph/dot_general | solution.py:54
  16.1 2.4 %reduce-window.6 = f32[2,4,3,128]{3,2,1,0:T(4,128)S(1)} reduce-window(f32[2,4,3,128]{3,2,1,0:T(4,128)S(1)} %copy.21, f32[]{:T(128)} %constant.74.clone.1), window={size=1x1x1x128 pad=0_0x0_0x0_0x127_0}, to_apply=%region_1.2 | reduce-window | flops 390144 | bytes 24580 | tf_op jit(solution)/shard_map/reduce-window
  18.5 0.1 slice.12
  18.6 0.1 copy.22
  18.8 0.1 copy.23
  18.9 0.1 broadcast_add_fusion
  19.0 0.2 slice_reduce_fusion
  19.1 0.1 copy.24
  19.2 22.3 %all-gather = f32[16,1,4]{2,1,0:T(1,128)S(1)} all-gather(f32[2,1,4]{2,1,0:T(1,128)S(1)} %copy.24), channel_id=2, replica_groups=mesh['sp'=8,'tp'=4] {'sp'}, dimensions={0}, use_global_device_ids=true | all-gather | bytes 288 | tf_op jit(solution)/shard_map/all_gather | solution.py:14
  41.5 0.3 while.16
  41.8 0.0 copy-done.6
  41.8 4.7 %fusion.91 = (f32[2,4]{1,0:T(2,128)S(1)}, f32[2,384,4]{1,2,0:T(4,128)S(1)}) fusion(bf16[4096,16]{0,1:T(8,128)(2,1)S(1)} %copy-done.6, s32[]{:T(128)S(6)} %select_n.52, bf16[2,384,4096]{2,1,0:T(8,128)(2,1)} %param.10, f32[2,384]{1,0:T(2,128)S(1)} %add_rsqrt_fusion, f32[2,4,384]{2,1,0:T(4,128)S(1)} %reduce_window_sum.16, f32[2,4]{1,0:T(2,128)S(1)} %add.125), kind=kOutput, calls=%fused_computation.73 | convolution fusion | flops 34612216 | bytes 6352932 | tf_op jit(solution)/shard_map/spd,dh->sph/dot_general | solution.py:52
  46.5 17.1 %pmax.7 = f32[2,4]{1,0:T(2,128)S(1)} all-reduce(f32[2,4]{1,0:T(2,128)S(1)} %get-tuple-element.143), channel_id=1, replica_groups=mesh['sp'=8,'tp'=4] {'sp'}, use_global_device_ids=true, to_apply=%region_6.7 | all-reduce | flops 8 | bytes 64 | tf_op jit(solution)/shard_map/pmax | solution.py:61
  63.6 0.0 copy-start.4
  63.6 7.5 %fusion.27 = bf16[2,48,4,8,128]{4,3,2,1,0:T(8,128)(2,1)S(1)} fusion(bf16[4096,512]{1,0:T(8,128)(2,1)} %param.11, bf16[2,384,4096]{2,1,0:T(8,128)(2,1)} %param.10, f32[2,384]{1,0:T(2,128)S(1)} %add_rsqrt_fusion), kind=kOutput, calls=%fused_computation.15 | convolution fusion | flops 3231055872 | bytes 11275264 | tf_op jit(solution)/shard_map/spd,dc->spc/dot_general | solution.py:46
  71.1 0.0 copy-start.1
  71.1 0.1 fusion.98
  71.2 0.8 copy-done.1
  72.0 0.2 fusion.48
  72.2 0.2 copy.32
  72.4 0.7 reshape.91
  73.1 0.0 reduce-scatter.7.cloned.1.call-update
  73.2 0.0 reduce-scatter.5.cloned.1.call-start
  73.2 0.1 subtract_exponential_fusion
  73.3 6.9 %fusion.17 = f32[2,384,512]{2,1,0:T(8,128)S(1)} fusion(bf16[4096,512]{1,0:T(8,128)(2,1)} %param.12, bf16[2,384,4096]{2,1,0:T(8,128)(2,1)} %param.10, f32[2,384]{1,0:T(2,128)S(1)} %add_rsqrt_fusion), kind=kOutput, calls=%fused_computation.13 | convolution fusion | flops 3231449088 | bytes 12061696 | tf_op jit(solution)/shard_map/spd,dc->spc/dot_general | solution.py:49
  80.2 0.0 copy-start.5
  80.2 0.5 copy.31
  80.7 2.3 %fusion.47 = f32[2,4,128,128]{3,2,1,0:T(8,128)} fusion(f32[2,384,4,128]{1,3,2,0:T(8,128)S(1)} %bitcast.61, f32[2,384,4]{1,2,0:T(4,128)S(1)} %subtract_exponential_fusion, bf16[2,48,4,8,128]{4,3,2,1,0:T(8,128)(2,1)} %copy-done.1), kind=kOutput, calls=%fused_computation.27 | convolution fusion | flops 101449728 | bytes 2895872 | tf_op jit(solution)/shard_map/sthe,sthd->shed/dot_general | solution.py:67
  83.0 0.0 reduce-scatter.5.cloned.1.call-update
  83.0 0.0 copy-done.5
  83.0 5.2 %all_gather.7 = bf16[2,4096]{1,0:T(2,128)(2,1)S(1)} all-gather(bf16[2,1024]{1,0:T(2,128)(2,1)S(1)} %copy-done.5), channel_id=1, replica_groups=mesh['sp'=8,'tp'=4] {'tp'}, dimensions={1}, use_global_device_ids=true | all-gather | bytes 20480 | tf_op jit(solution)/shard_map/all_gather | solution.py:75
  88.2 0.1 fusion.54
  88.4 2.9 %fusion.45 = f32[2,512]{1,0:T(2,128)S(1)} fusion(bf16[4096,512]{1,0:T(8,128)(2,1)} %param.11, bf16[2,4096]{1,0:T(2,128)(2,1)S(1)} %all_gather.7, f32[2]{0:T(128)S(1)} %add_rsqrt_fusion.1), kind=kOutput, calls=%fused_computation.23 | convolution fusion | flops 8415232 | bytes 4214792 | tf_op jit(solution)/shard_map/dot_general | solution.py:79
  91.3 2.9 %convolution_convert_fusion.2 = bf16[2,512]{1,0:T(2,128)(2,1)S(1)} fusion(bf16[4096,512]{1,0:T(8,128)(2,1)} %param.13, bf16[2,4096]{1,0:T(2,128)(2,1)S(1)} %all_gather.7, f32[2]{0:T(128)S(1)} %add_rsqrt_fusion.1), kind=kOutput, calls=%fused_computation.24 | convolution fusion | flops 8414208 | bytes 4212744 | tf_op jit(solution)/shard_map/dot_general | solution.py:76
  94.2 0.1 multiply_reduce_fusion.1
  94.3 0.2 fusion.58
  94.5 2.9 %fusion.44 = f32[2,512]{1,0:T(2,128)S(1)} fusion(bf16[4096,512]{1,0:T(8,128)(2,1)} %param.12, bf16[2,4096]{1,0:T(2,128)(2,1)S(1)} %all_gather.7, f32[2]{0:T(128)S(1)} %add_rsqrt_fusion.1), kind=kOutput, calls=%fused_computation.21 | convolution fusion | flops 8415232 | bytes 4214792 | tf_op jit(solution)/shard_map/dot_general | solution.py:80
  97.4 37.1 %reduce-scatter.7.cloned.1.call-done = f32[16,8]{1,0:T(8,128)} async-done(((f32[128,8]{1,0:T(8,128)}), f32[16,8]{1,0:T(8,128)}) %reduce-scatter.7.cloned.1.call-update) | async-done | bytes 528
  134.6 0.8 reshape.92
  135.3 0.1 copy.33
  135.4 0.0 copy-start.3
  135.4 0.2 multiply_reduce_fusion
  135.6 19.5 %psum.7 = f32[2,4]{1,0:T(2,128)S(1)} all-reduce(f32[2,4]{1,0:T(2,128)S(1)} %multiply_reduce_fusion), channel_id=1, replica_groups=mesh['sp'=8,'tp'=4] {'sp'}, use_global_device_ids=true, to_apply=%region_12.13 | all-reduce | flops 8 | bytes 64 | tf_op jit(solution)/shard_map/psum | solution.py:101
  155.1 0.0 copy-done.4
  155.1 0.2 abs_maximum_fusion
  155.4 44.3 %reduce-scatter.5.cloned.1.call-done = f32[2,4,16,128]{3,2,1,0:T(8,128)} async-done(((f32[2,4,128,128]{3,2,1,0:T(8,128)}), f32[2,4,16,128]{3,2,1,0:T(8,128)}) %reduce-scatter.5.cloned.1.call-update) | async-done | bytes 65552 | tf_op jit(solution)/shard_map/reduce_scatter | solution.py:71
  199.7 0.8 convert_element_type.54
  200.5 0.0 copy-start.2
  200.5 0.1 fusion.92
  200.6 0.7 fusion.70
  201.3 0.0 copy-done.3
  201.3 0.0 copy-done.2
  (21 shorter events, 0.2 us)
Async XLA Ops:
  7.2 4.3 %copy-start = (bf16[4096,16]{0,1:T(8,128)(2,1)S(1)}, bf16[4096,16]{0,1:T(8,128)(2,1)}, u32[]{:S(2)}) copy-start(bf16[4096,16]{0,1:T(8,128)(2,1)} %param.15) | copy-start | bytes 393220
  7.2 4.2 %copy-start.7 = (f32[16]{0:T(128)S(1)}, f32[16]{0:T(128)}, u32[]{:S(2)}) copy-start(f32[16]{0:T(128)} %param.16) | copy-start | bytes 196
  7.2 127.4 %reduce-scatter.7.cloned.1.call-start = ((), (), s32[]{:S(2)}) async-start(), calls=%async_computation.3 | async-start | bytes 73728
  7.2 34.6 %copy-start.6 = (bf16[4096,16]{0,1:T(8,128)(2,1)S(1)}, bf16[4096,16]{0,1:T(8,128)(2,1)}, u32[]{:S(2)}) copy-start(bf16[4096,16]{0,1:T(8,128)(2,1)} %param.14) | copy-start | bytes 393220
  63.6 91.5 %copy-start.4 = (f32[2,4]{1,0:T(2,128)}, f32[2,4]{1,0:T(2,128)S(1)}, u32[]{:S(2)}) copy-start(f32[2,4]{1,0:T(2,128)S(1)} %pmax.7) | copy-start | bytes 100
  71.1 0.9 copy-start.1
  73.2 126.5 %reduce-scatter.5.cloned.1.call-start = ((), (), s32[]{:S(2)}) async-start(), calls=%async_computation.2 | async-start | bytes 589824 | tf_op jit(solution)/shard_map/reduce_scatter | solution.py:71
  80.2 2.8 %copy-start.5 = (bf16[2,1024]{1,0:T(2,128)(2,1)S(1)}, bf16[2,1024]{1,0:T(2,128)(2,1)}, u32[]{:S(2)}) copy-start(bf16[2,1024]{1,0:T(2,128)(2,1)} %param.17) | copy-start | bytes 12292
  135.4 65.9 %copy-start.3 = (f32[2,4,16]{2,1,0:T(4,128)}, f32[2,4,16]{2,1,0:T(4,128)S(1)}, u32[]{:S(2)}) copy-start(f32[2,4,16]{2,1,0:T(4,128)S(1)} %copy.33) | copy-start | bytes 1540
  200.5 0.8 copy-start.2
Sparse Core Ops, SparseCore 0:
  73.3 61.2 reduce-scatter.6
  137.9 61.7 reduce-scatter.4
where the time goes:
time: 209 us; the launch traced here: 208 us
  waiting for transfers between devices  81.5 us (39%)
  blocking collectives  64.1 us (31%)
  matrix products  35.4 us (17%)
  between operations  14.2 us (7%)
  other arithmetic  8.84 us (4%)
  local copies, waits for them, and re-layouts  3.79 us (2%)
    reduce_scatter x1, waiting for transfers between devices, shards(): lax.psum_scatter(partial_matrix, 'sp', scatter_dimension=2, tiled=True)  44.3 us
    unnamed x3, waiting for transfers between devices  37.2 us
    all_gather x1, blocking collectives, prefix(): everything = lax.all_gather(value, axis)  22.3 us
    psum x1, blocking collectives, shards(): normal_dot = lax.psum(jnp.sum(normal * query_own, axis=-1), 'sp')  19.5 us
    pmax x1, blocking collectives, shards(): stabilizer = lax.pmax(jnp.max(log_weight, axis=1), 'sp')  17.1 us
    dot_general x1, matrix products, shards(): jnp.einsum('spd,dc->spc', normed, w_key, preferred_element_type=jnp.float32)  7.46 us
    dot_general x1, matrix products, shards(): jnp.einsum('spd,dc->spc', normed, w_value, preferred_element_type=jnp.flo...  6.89 us
    all_gather x1, blocking collectives, shards(): new_normed = normalize(lax.all_gather(new_rows, 'tp', axis=1, tiled=True))  5.21 us
  transfers between devices with their start and end apart: 2, of which 2 were waited for; matrix products, arithmetic and copies ran while one was open for 10% of the time, Pallas kernels for 0%

commit v1 on v0

v1 whole, which is shorter than its diff:
```python
import functools

import jax
import jax.numpy as jnp
from jax import lax
from jax.experimental import pallas as pl
from jax.experimental.pallas import tpu as pltpu
from jax.sharding import PartitionSpec as P

DH = 128
EPS = 1e-06
ROWS = 8
F32, BF16 = jnp.float32, jnp.bfloat16


def log1p_unit(u):
    z = u / (2.0 + u)
    q = z * z
    tail = jnp.full_like(q, 1.0 / 17)
    for odd in (15, 13, 11, 9, 7, 5, 3, 1):
        tail = tail * q + 1.0 / odd
    return 2.0 * z * tail


def log_sigmoid(x):
    return jnp.minimum(x, 0.0) - log1p_unit(jnp.exp(-jnp.abs(x)))


def normalize(rows):
    scaled = rows.astype(F32)
    mean = jnp.mean(scaled * scaled, axis=-1, keepdims=True)
    return (scaled * lax.rsqrt(mean + EPS)).astype(BF16)


def kernel(
    n, t, x_hbm, wk_hbm, wv_hbm, wq_hbm, wi_hbm, wf_hbm, bias_ref, new_hbm,
    mat_out, normal_out, top_out, read_out,
    x, wk, wv, wq, wi, wf, gw, gates, gates_new, keys, values, new_src, new_all, new_x,
    token, send, recv, stat_send, stat_recv,
    load_sem, new_send, new_recv, mat_send_sem, mat_recv_sem, stat_send_sem, stat_recv_sem,
):
    me, tp = lax.axis_index("sp"), lax.axis_index("tp")
    seqs, span, width = x.shape
    columns = wk.shape[1]
    heads = columns // DH
    all_heads = wi.shape[1]
    own = DH // n
    head_start = tp * heads
    up = lax.rem(2 * all_heads - head_start, 2 * all_heads)

    barrier = pltpu.get_barrier_semaphore()
    for k in range(1, n):
        pl.semaphore_signal(
            barrier, inc=1, device_id=(lax.rem(me + k, n), tp),
            device_id_type=pl.DeviceIdType.MESH)
    for k in range(1, t):
        pl.semaphore_signal(
            barrier, inc=1, device_id=(me, lax.rem(tp + k, t)),
            device_id_type=pl.DeviceIdType.MESH)

    pairs = [(new_hbm, new_src), (wi_hbm, wi), (wf_hbm, wf), (x_hbm.at[0], x.at[0]),
             (wk_hbm, wk), (wv_hbm, wv)]
    pairs += [(x_hbm.at[s], x.at[s]) for s in range(1, seqs)]
    pairs += [(wq_hbm, wq)]
    loads = [pltpu.make_async_copy(a, b, load_sem.at[i]) for i, (a, b) in enumerate(pairs)]
    for load in loads:
        load.start()
    new_load, wi_load, wf_load = loads[:3]
    x_loads = [loads[3]] + loads[6:6 + seqs - 1]
    wk_load, wv_load, wq_load = loads[4], loads[5], loads[-1]

    later = lax.broadcasted_iota(jnp.int32, (span, span), 0)
    earlier = lax.broadcasted_iota(jnp.int32, (span, span), 1)
    strict = (later > earlier).astype(F32).astype(BF16)
    head_row = lax.broadcasted_iota(jnp.int32, (ROWS, 1), 0)
    bias = jnp.zeros((ROWS, 1), F32)
    for h in range(heads):
        bias = jnp.where(head_row == h, bias_ref[head_start + h], bias)

    wi_load.wait()
    wf_load.wait()
    gw[...] = jnp.concatenate(
        [wi[...], wf[...], jnp.zeros((width, DH - 2 * all_heads), BF16)], axis=1)

    new_load.wait()
    pl.semaphore_wait(barrier, n - 1 + t - 1)
    new_copies = []
    for k in range(1, t):
        copy = pltpu.make_async_remote_copy(
            src_ref=new_src, dst_ref=new_all.at[tp],
            send_sem=new_send.at[k - 1], recv_sem=new_recv.at[k - 1],
            device_id=(me, lax.rem(tp + k, t)), device_id_type=pl.DeviceIdType.MESH)
        copy.start()
        new_copies.append(copy)
    new_all[tp] = new_src[...]

    block = 32 if span % 32 == 0 else span
    wide = 256 if columns % 256 == 0 else columns
    copies = []
    for s in range(seqs):
        x_loads[s].wait()

        def norm_step(i, carry):
            rows = pl.ds(pl.multiple_of(i * block, block), block)
            x[s, rows, :] = normalize(x[s, rows, :])
            return carry

        lax.fori_loop(0, span // block, norm_step, 0)

        gates[...] = jnp.dot(x[s], gw[...], preferred_element_type=F32).T
        own_gates = pltpu.roll(gates[:2 * all_heads, :], up, 0)
        igate = own_gates[:ROWS]
        logf = log_sigmoid(own_gates[all_heads:all_heads + ROWS] + bias)
        high = logf.astype(BF16).astype(F32)
        middle = (logf - high).astype(BF16).astype(F32)
        low = logf - high - middle
        parts = jnp.concatenate([high, middle, low, jnp.zeros_like(low)], axis=0).astype(BF16)
        sums = jnp.dot(parts, strict, preferred_element_type=F32)
        suffix = sums[:ROWS] + sums[ROWS:2 * ROWS] + sums[2 * ROWS:3 * ROWS]
        total = suffix[:, :1] + logf[:, :1]
        log_weight = suffix + igate
        top = jnp.max(log_weight, axis=1, keepdims=True)
        weight = jnp.exp(log_weight - top).T

        if s == 0:
            wk_load.wait()
            wv_load.wait()

        def project(c, carry):
            cols = pl.ds(pl.multiple_of(c * wide, wide), wide)
            keys[:, cols] = jnp.dot(x[s], wk[:, cols], preferred_element_type=F32).astype(BF16)
            values[:, cols] = jnp.dot(x[s], wv[:, cols], preferred_element_type=F32).astype(BF16)
            return carry

        lax.fori_loop(0, columns // wide, project, 0)

        lane = lax.broadcasted_iota(jnp.int32, (ROWS, DH), 1)
        stat_send[s, :ROWS, :] = jnp.zeros((ROWS, DH), F32)
        stat_send[s, ROWS:, :] = jnp.where(lane < DH // 2, top, total)
        for h in range(heads):
            share = weight[:, h:h + 1]
            key = keys[:, h * DH:(h + 1) * DH]
            value = values[:, h * DH:(h + 1) * DH]
            stat_send[s, h:h + 1, :] = jnp.sum(share * key.astype(F32), axis=0, keepdims=True)
            weighted = (share * value.astype(F32)).astype(BF16)
            part = lax.dot_general(
                weighted, key, (((0,), (0,)), ((), ())), preferred_element_type=F32)
            for j in range(n):
                send[s, j, h * own:(h + 1) * own, :] = part[j * own:(j + 1) * own].astype(send.dtype)
        for k in range(1, n):
            target = lax.rem(me + k, n)
            slot = s * (n - 1) + k - 1
            stat_copy = pltpu.make_async_remote_copy(
                src_ref=stat_send.at[s], dst_ref=stat_recv.at[s, me],
                send_sem=stat_send_sem.at[slot], recv_sem=stat_recv_sem.at[slot],
                device_id=(target, tp), device_id_type=pl.DeviceIdType.MESH)
            mat_copy = pltpu.make_async_remote_copy(
                src_ref=send.at[s, target], dst_ref=recv.at[s, me],
                send_sem=mat_send_sem.at[slot], recv_sem=mat_recv_sem.at[slot],
                device_id=(target, tp), device_id_type=pl.DeviceIdType.MESH)
            stat_copy.start()
            mat_copy.start()
            copies.append((s, stat_copy, mat_copy))
        stat_recv[s, me] = stat_send[s]
        recv[s, me] = send[s, me]

    for copy in new_copies:
        copy.wait()
    fresh = jnp.concatenate([new_all[i] for i in range(t)], axis=1)
    new_x[...] = jnp.zeros_like(new_x)
    new_x[:seqs, :] = normalize(fresh)
    rows = new_x[...]
    fresh_gates = jnp.dot(rows, gw[...], preferred_element_type=F32)
    gates_new[...] = jnp.concatenate(
        [fresh_gates, jnp.zeros((DH - 16, DH), F32)], axis=0).T
    wq_load.wait()
    token[...] = jnp.zeros_like(token)
    for which, w in enumerate((wq, wk, wv)):
        made = jnp.dot(rows, w[...], preferred_element_type=F32).astype(BF16).astype(F32)
        for s in range(seqs):
            for h in range(heads):
                token[which, s, h:h + 1, :] = made[s:s + 1, h * DH:(h + 1) * DH]
    own_new = pltpu.roll(gates_new[:2 * all_heads, :], up, 0)
    factor = DH ** (-0.5)
    turn = lax.rem(DH - me * own, DH)
    for s in range(seqs):
        query, key, value = token[0, s], token[1, s], token[2, s]
        igate_new = own_new[:ROWS, s:s + 1]
        logf_new = log_sigmoid(own_new[all_heads:all_heads + ROWS, s:s + 1] + bias)
        agreement = jnp.sum(key * query, axis=1, keepdims=True)
        value_own = pltpu.roll(value, turn, 1)[:, :own]

        for at, stat_copy, mat_copy in copies:
            if at == s:
                stat_copy.wait()
        beyond = jnp.zeros((ROWS, 1), F32)
        tops = [None] * n
        for j in reversed(range(n)):
            stat = stat_recv[s, j, ROWS:, :]
            tops[j] = beyond + stat[:, :1]
            beyond = beyond + stat[:, DH // 2:DH // 2 + 1]
        stabilizer = functools.reduce(jnp.maximum, tops)
        scales = [jnp.exp(top - stabilizer) for top in tops]
        normal = jnp.zeros((ROWS, DH), F32)
        for j in range(n):
            normal = normal + scales[j] * stat_recv[s, j, :ROWS, :]
        top_out[s] = jnp.broadcast_to(stabilizer, (ROWS, DH))
        normal_out[s] = pltpu.roll(normal, turn, 1)[:heads, :own]
        top_next = jnp.maximum(logf_new + stabilizer, igate_new)
        old_share = jnp.exp(logf_new + stabilizer - top_next)
        new_share = jnp.exp(igate_new - top_next)
        normal_dot = jnp.sum(normal * query, axis=1, keepdims=True)
        denominator = (old_share * normal_dot + new_share * agreement) * factor

        for at, stat_copy, mat_copy in copies:
            if at == s:
                mat_copy.wait()
        reading = jnp.zeros((ROWS, own), F32)
        query_low = query.astype(BF16)
        for h in range(heads):
            total = jnp.zeros((own, DH), F32)
            for j in range(n):
                piece = recv[s, j, h * own:(h + 1) * own, :].astype(F32)
                total = total + scales[j][h:h + 1, :] * piece
            stored = total.astype(BF16)
            mat_out[s, h] = stored
            seen = lax.dot_general(
                query_low, stored, (((1,), (1,)), ((), ())), preferred_element_type=F32)
            reading = jnp.where(head_row == h, seen, reading)
        numerator = (old_share * reading + (new_share * agreement) * value_own) * factor
        read = numerator / jnp.maximum(jnp.abs(denominator), 1.0)
        read_out[s] = read[:heads].astype(BF16)


def shards(n, t, inputs, w_key, w_value, w_query, w_igate, w_fgate, forget_bias, new_rows):
    seqs, span, width = inputs.shape
    columns = w_key.shape[1]
    heads = columns // DH
    own = DH // n
    all_heads = w_igate.shape[1]
    wire = BF16 if own % 16 == 0 else F32
    hbm = pl.BlockSpec(memory_space=pl.ANY)
    vmem = pl.BlockSpec(memory_space=pltpu.VMEM)
    scratch = [
        pltpu.VMEM((seqs, span, width), BF16),
        pltpu.VMEM((width, columns), BF16),
        pltpu.VMEM((width, columns), BF16),
        pltpu.VMEM((width, columns), BF16),
        pltpu.VMEM((width, all_heads), BF16),
        pltpu.VMEM((width, all_heads), BF16),
        pltpu.VMEM((width, DH), BF16),
        pltpu.VMEM((DH, span), F32),
        pltpu.VMEM((DH, DH), F32),
        pltpu.VMEM((span, columns), BF16),
        pltpu.VMEM((span, columns), BF16),
        pltpu.VMEM(new_rows.shape, BF16),
        pltpu.VMEM((t,) + new_rows.shape, BF16),
        pltpu.VMEM((16, width), BF16),
        pltpu.VMEM((3, seqs, ROWS, DH), F32),
        pltpu.VMEM((seqs, n, heads * own, DH), wire),
        pltpu.VMEM((seqs, n, heads * own, DH), wire),
        pltpu.VMEM((seqs, 2 * ROWS, DH), F32),
        pltpu.VMEM((seqs, n, 2 * ROWS, DH), F32),
        pltpu.SemaphoreType.DMA((7 + seqs - 1,)),
        pltpu.SemaphoreType.DMA((t - 1,)),
        pltpu.SemaphoreType.DMA((t - 1,)),
        pltpu.SemaphoreType.DMA((seqs * (n - 1),)),
        pltpu.SemaphoreType.DMA((seqs * (n - 1),)),
        pltpu.SemaphoreType.DMA((seqs * (n - 1),)),
        pltpu.SemaphoreType.DMA((seqs * (n - 1),)),
    ]
    matrix, normal, top, read = pl.pallas_call(
        functools.partial(kernel, n, t),
        out_shape=(
            jax.ShapeDtypeStruct((seqs, heads, own, DH), BF16),
            jax.ShapeDtypeStruct((seqs, heads, own), F32),
            jax.ShapeDtypeStruct((seqs, ROWS, DH), F32),
            jax.ShapeDtypeStruct((seqs, heads, own), BF16),
        ),
        in_specs=[hbm] * 6 + [pl.BlockSpec(memory_space=pltpu.SMEM), hbm],
        out_specs=(vmem,) * 4,
        scratch_shapes=scratch,
        compiler_params=pltpu.CompilerParams(
            collective_id=0, has_side_effects=True, vmem_limit_bytes=60 * 1024 * 1024),
    )(inputs, w_key, w_value, w_query, w_igate, w_fgate, forget_bias, new_rows)
    return matrix, normal, top[:, :heads, 0], read


def solution(mesh):
    in_specs = (
        P(None, "sp", None),
        P(None, "tp"),
        P(None, "tp"),
        P(None, "tp"),
        P(),
        P(),
        P(),
        P(None, "tp"),
    )
    out_specs = (P(None, "tp", "sp", None), P(None, "tp", "sp"), P(None, "tp"), P(None, "tp", "sp"))
    body = functools.partial(shards, mesh.shape["sp"], mesh.shape["tp"])
    return jax.shard_map(body, mesh=mesh, in_specs=in_specs, out_specs=out_specs, check_vma=False)
```

time: 209 us -> 39.3 us (0.19)
  waiting for transfers between devices: 81.5 us -> 0 us
  blocking collectives: 64.1 us -> 0 us
  matrix products: 35.4 us -> 0 us
  Pallas kernels: 0 us -> 28.5 us
  between operations: 14.2 us -> 0.64 us
  other arithmetic: 8.84 us -> 0 us
  local copies, waits for them, and re-layouts: 3.79 us -> 9.76 us
    reduce_scatter x1 -> x0, waiting for transfers between devices: 44.3 us -> none  [shards(): lax.psum_scatter(partial_matrix, 'sp', scatter_dimension=2, tiled=True)]
    unnamed x3 -> x0, waiting for transfers between devices: 37.2 us -> none
    dot_general x12 -> x0, matrix products: 35.4 us -> none  [the longest x1 7.46 us: shards(): jnp.einsum('spd,dc->spc', normed, w_key, preferred_element_type=jnp.float32)]
    pallas_call x0 -> x1, Pallas kernels: none -> 28.5 us  [shards(): pl.pallas_call(functools.partial(kernel, n, t), out_shape=(jax.ShapeDtype...]
    all_gather x2 -> x0, blocking collectives: 27.5 us -> none  [the longest x1 22.3 us: prefix(): everything = lax.all_gather(value, axis)]
    psum x1 -> x0, blocking collectives: 19.5 us -> none  [shards(): normal_dot = lax.psum(jnp.sum(normal * query_own, axis=-1), 'sp')]
    pmax x1 -> x0, blocking collectives: 17.1 us -> none  [shards(): stabilizer = lax.pmax(jnp.max(log_weight, axis=1), 'sp')]
    unnamed x20 -> x5, local copies, waits for them, and re-layouts: 2.61 us -> 8.41 us
  transfers between devices with their start and end apart: 2 -> 0, of which waited for: 2 -> 0; matrix products, arithmetic and copies ran while one was open for 10% -> 0% of each run, Pallas kernels for 0% -> 0%
where the time goes in v1:
time: 39.3 us; the launch traced here: 38.9 us
  Pallas kernels  28.5 us (73%)
  local copies, waits for them, and re-layouts  9.76 us (25%)
  between operations  0.64 us (2%)
    pallas_call x1, Pallas kernels, shards(): pl.pallas_call(functools.partial(kernel, n, t), out_shape=(jax.ShapeDtype...  28.5 us
    unnamed x5, local copies, waits for them, and re-layouts  8.41 us
    slice x1, local copies, waits for them, and re-layouts, shards(): return (matrix, normal, top[:, :heads, 0], read)  1.35 us

profile of v1, /device:TPU:0, one launch (start us, length us, event | category | flops | bytes accessed | tf_op | source)
XLA Modules:
  0.0 38.9 jit_solution(6052152584434938535)
XLA Ops:
  0.6 2.2 %copy.14.wi_hbm = bf16[4096,16]{1,0:T(8,128)(2,1)} copy(bf16[4096,16]{0,1:T(8,128)(2,1)} %param.12) | data formatting | bytes 262144 | tf_op args[4]
  2.9 2.3 %copy.15.wf_hbm = bf16[4096,16]{1,0:T(8,128)(2,1)} copy(bf16[4096,16]{0,1:T(8,128)(2,1)} %param.13) | data formatting | bytes 262144 | tf_op args[5]
  5.2 28.5 %shard_map.111 = (bf16[2,4,16,128]{3,2,1,0:T(8,128)(2,1)}, f32[2,4,16]{2,1,0:T(4,128)}, f32[2,8,128]{2,1,0:T(8,128)}, bf16[2,4,16]{2,1,0:T(4,128)(2,1)}) custom-call(bf16[2,384,4096]{2,1,0:T(8,128)(2,1)} %x_hbm.1, bf16[4096,512]{1,0:T(8,128)(2,1)} %wk_hbm.1, bf16[4096,512]{1,0:T(8,128)(2,1)} %wv_hbm.1, bf16[4096,512]{1,0:T(8,128)(2,1)} %wq_hbm.1, ...), custom_call_target="tpu_custom_call" | custom-call | tf_op jit(solution)/shard_map/pallas_call | solution.py:272
  33.7 1.3 %slice_reduce_fusion = f32[2,4]{1,0:T(2,128)} fusion(f32[2,8,128]{2,1,0:T(8,128)} %get-tuple-element.10), kind=kLoop, calls=%fused_computation | loop fusion | bytes 64 | tf_op jit(solution)/shard_map/slice | solution.py:286
  35.0 1.4 %copy.19 = bf16[2,4,16,128]{3,2,1,0:T(8,128)(2,1)} copy(bf16[2,4,16,128]{3,2,1,0:T(8,128)(2,1)} %get-tuple-element.16) | data formatting | bytes 65536
  36.4 1.3 %copy.20 = f32[2,4,16]{2,1,0:T(4,128)} copy(f32[2,4,16]{2,1,0:T(4,128)} %get-tuple-element.17) | data formatting | bytes 1024
  37.7 1.2 %copy.21 = bf16[2,4,16]{2,1,0:T(4,128)(2,1)} copy(bf16[2,4,16]{2,1,0:T(4,128)(2,1)} %get-tuple-element.19) | data formatting | bytes 512

commit v2 on v1

v2 whole, which is shorter than its diff:
```python
import functools

import jax
import jax.numpy as jnp
from jax import lax
from jax.experimental import pallas as pl
from jax.experimental.pallas import tpu as pltpu
from jax.sharding import PartitionSpec as P

DH = 128
EPS = 1e-06
ROWS = 8
F32, BF16 = jnp.float32, jnp.bfloat16


def log1p_unit(u):
    z = u / (2.0 + u)
    q = z * z
    tail = jnp.full_like(q, 1.0 / 17)
    for odd in (15, 13, 11, 9, 7, 5, 3, 1):
        tail = tail * q + 1.0 / odd
    return 2.0 * z * tail


def log_sigmoid(x):
    return jnp.minimum(x, 0.0) - log1p_unit(jnp.exp(-jnp.abs(x)))


def normalize(rows):
    scaled = rows.astype(F32)
    mean = jnp.mean(scaled * scaled, axis=-1, keepdims=True)
    return (scaled * lax.rsqrt(mean + EPS)).astype(BF16)


def kernel(
    n, t, x_hbm, wk_hbm, wv_hbm, wq_hbm, wi_hbm, wf_hbm, bias_ref, new_hbm,
    mat_out, normal_out, top_out, read_out,
    x, wk, wv, wq, gw_rows, gw, gates_new, new_src, new_all, new_x,
    strict, token, send, recv, normal_send, normal_recv,
    load_sem, new_send, new_recv, mat_send_sem, mat_recv_sem,
    normal_send_sem, normal_recv_sem,
):
    me, tp = lax.axis_index("sp"), lax.axis_index("tp")
    seqs, span, width = x.shape
    columns = wk.shape[1]
    heads = columns // DH
    all_heads = wi_hbm.shape[0]
    own = DH // n
    head_start = tp * heads
    up = lax.rem(2 * all_heads - head_start, 2 * all_heads)
    wide = 256 if columns % 256 == 0 else columns
    chunks = columns // wide
    chunk_heads = wide // DH
    peers = [lax.rem(me + k, n) for k in range(1, n)]

    barrier = pltpu.get_barrier_semaphore()
    for peer in peers:
        pl.semaphore_signal(
            barrier, inc=1, device_id=(peer, tp), device_id_type=pl.DeviceIdType.MESH)
    for k in range(1, t):
        pl.semaphore_signal(
            barrier, inc=1, device_id=(me, lax.rem(tp + k, t)),
            device_id_type=pl.DeviceIdType.MESH)

    piece = 128 if span % 128 == 0 else span
    pieces = span // piece
    pairs = [(new_hbm, new_src), (wi_hbm, gw_rows.at[pl.ds(0, all_heads)]),
             (wf_hbm, gw_rows.at[pl.ds(all_heads, all_heads)])]
    pairs += [(x_hbm.at[0, pl.ds(i * piece, piece)], x.at[0, pl.ds(i * piece, piece)])
              for i in range(pieces)]
    pairs += [(wk_hbm, wk), (wv_hbm, wv)]
    pairs += [(x_hbm.at[s], x.at[s]) for s in range(1, seqs)]
    pairs += [(wq_hbm, wq)]
    loads = [pltpu.make_async_copy(a, b, load_sem.at[i]) for i, (a, b) in enumerate(pairs)]
    for load in loads:
        load.start()
    new_load, wi_load, wf_load = loads[:3]
    first_loads = loads[3:3 + pieces]
    wk_load, wv_load = loads[3 + pieces:5 + pieces]
    x_loads = [None] + loads[5 + pieces:-1]
    wq_load = loads[-1]

    later = lax.broadcasted_iota(jnp.int32, (span, span), 0)
    earlier = lax.broadcasted_iota(jnp.int32, (span, span), 1)
    strict[...] = (later > earlier).astype(F32).astype(BF16)
    head_row = lax.broadcasted_iota(jnp.int32, (ROWS, 1), 0)
    lane = lax.broadcasted_iota(jnp.int32, (ROWS, DH), 1)
    bias = jnp.zeros((ROWS, 1), F32)
    for h in range(heads):
        bias = jnp.where(head_row == h, bias_ref[head_start + h], bias)

    block = 16 if span % 16 == 0 else span

    def norm_rows(s, start, stop):
        for at in range(start, stop, block):
            x[s, at:at + block, :] = normalize(x[s, at:at + block, :])

    def push(src, dst, send_sem, recv_sem, peer):
        copy = pltpu.make_async_remote_copy(
            src_ref=src, dst_ref=dst, send_sem=send_sem, recv_sem=recv_sem,
            device_id=(peer, tp), device_id_type=pl.DeviceIdType.MESH)
        copy.start()
        return copy

    wi_load.wait()
    wf_load.wait()
    gw[...] = jnp.concatenate(
        [gw_rows[...], jnp.zeros((DH - 2 * all_heads, width), BF16)], axis=0).T
    for i in range(pieces):
        first_loads[i].wait()
        norm_rows(0, i * piece, (i + 1) * piece)

    normal_copies, mat_copies, new_copies = {}, {}, []
    for s in range(seqs):
        if s == 0:
            wk_load.wait()
        gates = jnp.dot(x[s], gw[...], preferred_element_type=F32).T
        own_gates = pltpu.roll(gates[:2 * all_heads, :], up, 0)
        igate = own_gates[:ROWS]
        logf = log_sigmoid(own_gates[all_heads:all_heads + ROWS] + bias)
        high = logf.astype(BF16).astype(F32)
        middle = (logf - high).astype(BF16).astype(F32)
        low = logf - high - middle
        parts = jnp.concatenate([high, middle, low, jnp.zeros_like(low)], axis=0).astype(BF16)
        sums = jnp.dot(parts, strict[...], preferred_element_type=F32)
        suffix = sums[:ROWS] + sums[ROWS:2 * ROWS] + sums[2 * ROWS:3 * ROWS]
        total = suffix[:, :1] + logf[:, :1]
        log_weight = suffix + igate
        top = jnp.max(log_weight, axis=1, keepdims=True)
        weight = jnp.exp(log_weight - top)
        high = weight.astype(BF16).astype(F32)
        middle = (weight - high).astype(BF16).astype(F32)
        weights = jnp.concatenate(
            [high, middle, weight - high - middle, jnp.zeros_like(high)], axis=0).astype(BF16)
        stat = jnp.where(lane < DH // 2, top, total)
        normal_send[s, :ROWS, :] = jnp.zeros((ROWS, DH), F32)
        normal_send[s, ROWS:, :] = stat

        for c in range(chunks):
            cols = slice(c * wide, (c + 1) * wide)
            last = c == chunks - 1
            keys = jnp.dot(x[s], wk[:, cols], preferred_element_type=F32).astype(BF16)
            if s == 0 and c == 0:
                wv_load.wait()
                new_load.wait()
                pl.semaphore_wait(barrier, n - 1 + t - 1)
                for k in range(1, t):
                    copy = pltpu.make_async_remote_copy(
                        src_ref=new_src, dst_ref=new_all.at[tp],
                        send_sem=new_send.at[k - 1], recv_sem=new_recv.at[k - 1],
                        device_id=(me, lax.rem(tp + k, t)),
                        device_id_type=pl.DeviceIdType.MESH)
                    copy.start()
                    new_copies.append(copy)
                new_all[tp] = new_src[...]
            if last and s + 1 < seqs:
                x_loads[s + 1].wait()
                norm_rows(s + 1, 0, span)
            values = jnp.dot(x[s], wv[:, cols], preferred_element_type=F32).astype(BF16)
            sums = jnp.dot(weights, keys, preferred_element_type=F32)
            sums = sums[:ROWS] + sums[ROWS:2 * ROWS] + sums[2 * ROWS:3 * ROWS]
            flipped = values.T
            for i in range(chunk_heads):
                h = c * chunk_heads + i
                normal_send[s, h:h + 1, :] = sums[h:h + 1, i * DH:(i + 1) * DH]
                value = flipped[i * DH:(i + 1) * DH].astype(F32)
                weighted = (weight[h:h + 1, :] * value).astype(BF16)
                part = jnp.dot(
                    weighted, keys[:, i * DH:(i + 1) * DH], preferred_element_type=F32)
                for j in range(n):
                    send[s, j, c, i * own:(i + 1) * own, :] = (
                        part[j * own:(j + 1) * own].astype(send.dtype))
        normal_copies[s] = [
            push(normal_send.at[s], normal_recv.at[s, me],
                 normal_send_sem.at[s * (n - 1) + k], normal_recv_sem.at[s * (n - 1) + k],
                 peer) for k, peer in enumerate(peers)]
        normal_recv[s, me] = normal_send[s]
        mat_copies[s] = [
            push(send.at[s, peer], recv.at[s, me],
                 mat_send_sem.at[s * (n - 1) + k], mat_recv_sem.at[s * (n - 1) + k], peer)
            for k, peer in enumerate(peers)]
        recv[s, me] = send[s, me]

    for copy in new_copies:
        copy.wait()
    fresh = jnp.concatenate([new_all[i] for i in range(t)], axis=1)
    new_x[...] = jnp.zeros_like(new_x)
    new_x[:seqs, :] = normalize(fresh)
    rows = new_x[...]
    fresh_gates = jnp.dot(rows, gw[...], preferred_element_type=F32)
    gates_new[...] = jnp.concatenate(
        [fresh_gates, jnp.zeros((DH - 16, DH), F32)], axis=0).T
    wq_load.wait()
    token[...] = jnp.zeros_like(token)
    for which, w in enumerate((wq, wk, wv)):
        made = jnp.dot(rows, w[...], preferred_element_type=F32).astype(BF16).astype(F32)
        for s in range(seqs):
            for h in range(heads):
                token[which, s, h:h + 1, :] = made[s:s + 1, h * DH:(h + 1) * DH]
    own_new = pltpu.roll(gates_new[:2 * all_heads, :], up, 0)
    factor = DH ** (-0.5)
    turn = lax.rem(DH - me * own, DH)
    for s in range(seqs):
        query, key, value = token[0, s], token[1, s], token[2, s]
        igate_new = own_new[:ROWS, s:s + 1]
        logf_new = log_sigmoid(own_new[all_heads:all_heads + ROWS, s:s + 1] + bias)
        agreement = jnp.sum(key * query, axis=1, keepdims=True)
        value_own = pltpu.roll(value, turn, 1)[:, :own]

        for copy in normal_copies[s]:
            copy.wait()
        beyond = jnp.zeros((ROWS, 1), F32)
        tops = [None] * n
        for j in reversed(range(n)):
            stat = normal_recv[s, j, ROWS:, :]
            tops[j] = beyond + stat[:, :1]
            beyond = beyond + stat[:, DH // 2:DH // 2 + 1]
        stabilizer = functools.reduce(jnp.maximum, tops)
        scales = [jnp.exp(top - stabilizer) for top in tops]
        top_row = jnp.sum(jnp.where(lane == head_row, stabilizer, 0.0), axis=0, keepdims=True)
        top_out[s:s + 1, :] = top_row[:, :heads]
        top_next = jnp.maximum(logf_new + stabilizer, igate_new)
        old_share = jnp.exp(logf_new + stabilizer - top_next)
        new_share = jnp.exp(igate_new - top_next)
        reading = jnp.zeros((ROWS, own), F32)
        query_low = query.astype(BF16)
        for c in range(chunks):
            for copy in mat_copies[s] if c == 0 else ():
                copy.wait()
            for i in range(chunk_heads):
                h = c * chunk_heads + i
                total = jnp.zeros((own, DH), F32)
                for j in range(n):
                    part = recv[s, j, c, i * own:(i + 1) * own, :].astype(F32)
                    total = total + scales[j][h:h + 1, :] * part
                stored = total.astype(BF16)
                mat_out[s, h] = stored
                seen = lax.dot_general(
                    query_low, stored, (((1,), (1,)), ((), ())), preferred_element_type=F32)
                reading = jnp.where(head_row == h, seen, reading)
        normal = jnp.zeros((ROWS, DH), F32)
        for j in range(n):
            normal = normal + scales[j] * normal_recv[s, j, :ROWS, :]
        normal_out[s] = pltpu.roll(normal, turn, 1)[:heads, :own]
        normal_dot = jnp.sum(normal * query, axis=1, keepdims=True)
        denominator = (old_share * normal_dot + new_share * agreement) * factor
        numerator = (old_share * reading + (new_share * agreement) * value_own) * factor
        read = numerator / jnp.maximum(jnp.abs(denominator), 1.0)
        read_out[s] = read[:heads].astype(BF16)


def hand_on(*refs):
    count = (len(refs) - 2) // 3
    sources, targets, held = (refs[i * count:(i + 1) * count] for i in range(3))
    come, go = refs[-2:]
    ins = [pltpu.make_async_copy(a, b, come.at[i])
           for i, (a, b) in enumerate(zip(sources, held))]
    outs = [pltpu.make_async_copy(a, b, go.at[i])
            for i, (a, b) in enumerate(zip(held, targets))]
    for copy in ins:
        copy.start()
    for copy, on in zip(ins, outs):
        copy.wait()
        on.start()
    for on in outs:
        on.wait()


def shards(n, t, inputs, w_key, w_value, w_query, w_igate, w_fgate, forget_bias, new_rows):
    seqs, span, width = inputs.shape
    columns = w_key.shape[1]
    heads = columns // DH
    own = DH // n
    all_heads = w_igate.shape[1]
    wire = BF16 if own % 16 == 0 else F32
    hbm = pl.BlockSpec(memory_space=pl.ANY)
    vmem = pl.BlockSpec(memory_space=pltpu.VMEM)
    wide = 256 if columns % 256 == 0 else columns
    chunks = columns // wide
    slab = pltpu.VMEM((seqs, n, chunks, wide // DH * own, DH), wire)
    small = [pltpu.SemaphoreType.DMA((seqs * (n - 1),))] * 2
    scratch = [
        pltpu.VMEM((seqs, span, width), BF16),
        pltpu.VMEM((width, columns), BF16),
        pltpu.VMEM((width, columns), BF16),
        pltpu.VMEM((width, columns), BF16),
        pltpu.VMEM((2 * all_heads, width), BF16),
        pltpu.VMEM((width, DH), BF16),
        pltpu.VMEM((DH, DH), F32),
        pltpu.VMEM(new_rows.shape, BF16),
        pltpu.VMEM((t,) + new_rows.shape, BF16),
        pltpu.VMEM((16, width), BF16),
        pltpu.VMEM((span, span), BF16),
        pltpu.VMEM((3, seqs, ROWS, DH), F32),
        slab,
        slab,
        pltpu.VMEM((seqs, 2 * ROWS, DH), F32),
        pltpu.VMEM((seqs, n, 2 * ROWS, DH), F32),
        pltpu.SemaphoreType.DMA((5 + max(1, span // 128) + seqs,)),
        pltpu.SemaphoreType.DMA((t - 1,)),
        pltpu.SemaphoreType.DMA((t - 1,)),
        pltpu.SemaphoreType.DMA((seqs * (n - 1),)),
        pltpu.SemaphoreType.DMA((seqs * (n - 1),)),
    ] + small
    out_shape = (
        jax.ShapeDtypeStruct((seqs, heads, own, DH), BF16),
        jax.ShapeDtypeStruct((seqs, heads, own), F32),
        jax.ShapeDtypeStruct((seqs, heads), F32),
        jax.ShapeDtypeStruct((seqs, heads, own), BF16),
    )
    made = pl.pallas_call(
        functools.partial(kernel, n, t),
        out_shape=out_shape,
        in_specs=[hbm] * 6 + [pl.BlockSpec(memory_space=pltpu.SMEM), hbm],
        out_specs=(vmem,) * 4,
        scratch_shapes=scratch,
        compiler_params=pltpu.CompilerParams(
            collective_id=0, has_side_effects=True, vmem_limit_bytes=60 * 1024 * 1024),
    )(inputs, w_key, w_value, w_query, w_igate.T, w_fgate.T, forget_bias, new_rows)
    return pl.pallas_call(
        hand_on, out_shape=out_shape, in_specs=[hbm] * 4, out_specs=(hbm,) * 4,
        scratch_shapes=[pltpu.VMEM(out.shape, out.dtype) for out in out_shape]
        + [pltpu.SemaphoreType.DMA((4,))] * 2,
        compiler_params=pltpu.CompilerParams(vmem_limit_bytes=60 * 1024 * 1024),
    )(*made)


def solution(mesh):
    in_specs = (
        P(None, "sp", None),
        P(None, "tp"),
        P(None, "tp"),
        P(None, "tp"),
        P(),
        P(),
        P(),
        P(None, "tp"),
    )
    out_specs = (P(None, "tp", "sp", None), P(None, "tp", "sp"), P(None, "tp"), P(None, "tp", "sp"))
    body = functools.partial(shards, mesh.shape["sp"], mesh.shape["tp"])
    return jax.shard_map(body, mesh=mesh, in_specs=in_specs, out_specs=out_specs, check_vma=False)
```

time: 39.3 us -> 32.8 us (0.83)
  local copies, waits for them, and re-layouts: 9.76 us -> 0 us
  Pallas kernels: 28.5 us -> 32 us
    unnamed x5 -> x0, local copies, waits for them, and re-layouts: 8.41 us -> none
    pallas_call x1 -> x2, Pallas kernels: 28.5 us -> 32 us  [the longest x1 30.5 us: shards(): pl.pallas_call(functools.partial(kernel, n, t), out_shape=out_shape, in_s...]
    slice x1 -> x0, local copies, waits for them, and re-layouts: 1.35 us -> none  [shards(): return (matrix, normal, top[:, :heads, 0], read)]
where the time goes in v2:
time: 32.8 us; the launch traced here: 32.6 us
  Pallas kernels  32 us (98%)
  between operations  0.64 us (2%)
    pallas_call x1, Pallas kernels, shards(): pl.pallas_call(functools.partial(kernel, n, t), out_shape=out_shape, in_s...  30.5 us
    pallas_call x1, Pallas kernels, shards(): pl.pallas_call(hand_on, out_shape=out_shape, in_specs=[hbm] * 4, out_spec...  1.45 us

profile of v2, /device:TPU:0, one launch (start us, length us, event | category | flops | bytes accessed | tf_op | source)
XLA Modules:
  0.0 32.6 jit_solution(5440675073108834259)
XLA Ops:
  0.6 30.5 %shard_map.111 = (bf16[2,4,16,128]{3,2,1,0:T(8,128)(2,1)}, f32[2,4,16]{2,1,0:T(4,128)}, f32[2,4]{1,0:T(2,128)}, bf16[2,4,16]{2,1,0:T(4,128)(2,1)}) custom-call(bf16[2,384,4096]{2,1,0:T(8,128)(2,1)} %x_hbm.1, bf16[4096,512]{1,0:T(8,128)(2,1)} %wk_hbm.1, bf16[4096,512]{1,0:T(8,128)(2,1)} %wv_hbm.1, bf16[4096,512]{1,0:T(8,128)(2,1)} %wq_hbm.1, ...), custom_call_target="tpu_custom_call" | custom-call | tf_op jit(solution)/shard_map/pallas_call | solution.py:311
  31.2 1.4 %shard_map.112 = (bf16[2,4,16,128]{3,2,1,0:T(8,128)(2,1)}, f32[2,4,16]{2,1,0:T(4,128)}, f32[2,4]{1,0:T(2,128)}, bf16[2,4,16]{2,1,0:T(4,128)(2,1)}) custom-call(bf16[2,4,16,128]{3,2,1,0:T(8,128)(2,1)} %get-tuple-element.8.refs_0_, f32[2,4,16]{2,1,0:T(4,128)} %get-tuple-element.9.refs_1_, f32[2,4]{1,0:T(2,128)} %get-tuple-element.10.refs_2_, ...), custom_call_target="tpu_custom_call" | custom-call | tf_op jit(solution)/shard_map/pallas_call | solution.py:320
